TPU v7x, 256 devices: a whole 4x4x8 slice. The times are simulated.
256 devices in a mesh: sp: 32 (over z, x), tp: 8 (over y, core).
Axes of the slice: x: 4, y: 4, z: 8, core: 2. Of those that a mesh axis runs over, the one named last changes fastest.
Arguments:
- tokens: bfloat16 [24576, 4096], P('sp', 'tp'), may hold values from -6 to 6
- norm_gain: float32 [4096], replicated, may hold values from 0.1 to 1.9
- w_query: bfloat16 [4096, 2048], P('sp', 'tp'), may hold values from -0.09375 to 0.09375
- w_key: bfloat16 [4096, 1024], P('sp', 'tp'), may hold values from -0.09375 to 0.09375
- w_value: bfloat16 [4096, 1024], P('sp', 'tp'), may hold values from -0.09375 to 0.09375
- w_pool: bfloat16 [4096, 1024], P('sp', 'tp'), may hold values from -0.09375 to 0.09375
- query_gain: float32 [64], replicated, may hold values from 0.5 to 8
- key_gain: float32 [64], replicated, may hold values from 0.5 to 8
- sink_logit: float32 [32], P('tp'), may hold values from 1 to 5
- w_out_pool: bfloat16 [1024, 4096], P('tp', 'sp'), may hold values from -0.75 to 0.75
- w_out_attn: bfloat16 [2048, 4096], P('tp', 'sp'), may hold values from -1.5 to 1.5
Outputs:
- mixed: bfloat16 [24576, 4096], P(('sp', 'tp'))
All inputs are finite; a program needn't handle non-finite values.
Results may differ from a plain program's by a relative error of at most 0.014.
The roundings to bfloat16 on the way count: a program that leaves them out, or rounds other values in their place, can miss the bound.
Values may be sent and summed in bfloat16 or wider, within the bound.
No kernel may reach another device: no remote copies, remote signals or barrier semaphores. Data moves between devices by JAX's collectives and lax.ppermute only.
A program may use at most 128 MiB of HBM per device.

v0:
```python
import jax
import jax.numpy as jnp
from jax import lax
from jax.sharding import PartitionSpec as P

HEAD = 64
POOL = 1024
WINDOW = 128
GRID_W = 64
eps = 1e-06
rope_base = 10000.0
neg_big = -1e30
pool_reach = 8


def padded_2(block, sides, width):
    for axis, dim in sides:
        count = lax.axis_size(axis)
        forward = [(i, i + 1) for i in range(count - 1)]
        backward = [(target, source) for source, target in forward]
        low = lax.ppermute(
            lax.slice_in_dim(block, block.shape[dim] - width, None, axis=dim), axis, forward
        )
        high = lax.ppermute(lax.slice_in_dim(block, 0, width, axis=dim), axis, backward)
        block = jnp.concatenate([low, block, high], axis=dim)
    return block


def sent_together(arrays, axis, dim, along):
    ends, at = ([], 0)
    for a in arrays[:-1]:
        at += a.shape[along]
        ends.append(at)
    both = jnp.concatenate(arrays, axis=along)
    return tuple(jnp.split(lax.all_gather(both, axis, axis=dim, tiled=True), ends, axis=along))


def rope_tables(positions, head_size):
    quarter = head_size // 4
    freqs = 1.0 / rope_base ** (jnp.arange(quarter, dtype=jnp.float32) * 2.0 / (head_size // 2))
    row_angle = (positions // GRID_W).astype(jnp.float32)[:, None] * freqs
    col_angle = (positions % GRID_W).astype(jnp.float32)[:, None] * freqs
    angles = jnp.concatenate([row_angle, row_angle, col_angle, col_angle], axis=-1)
    return (jnp.cos(angles), jnp.sin(angles))


def rotate(heads_in, cosine, sine):
    part_one, part_two, part_three, part_four = jnp.split(heads_in, 4, axis=-1)
    turned = jnp.concatenate([-part_two, part_one, -part_four, part_three], axis=-1)
    return heads_in * cosine[:, None, :] + turned * sine[:, None, :]


def prepare(projected, gain, cosine, sine):
    rows_count = projected.shape[0]
    shaped = projected.reshape(rows_count, -1, HEAD)
    scaled = shaped * lax.rsqrt(jnp.mean(shaped * shaped, axis=-1, keepdims=True) + eps) * gain
    return rotate(scaled, cosine, sine).reshape(rows_count, -1).astype(jnp.bfloat16)


def edge_keys(keys_new, values_new):
    joined = jnp.concatenate([keys_new, values_new], axis=1)
    return padded_2(joined, (("sp", 0),), WINDOW)


def edge_pool(pool_in):
    return padded_2(pool_in, (("sp", 0),), pool_reach)


def window_attention(queries, key_band, sink_logit, positions, seq):
    rows_count = queries.shape[0]
    key_width = key_band.shape[1] // 2
    heads_q = queries.shape[1] // HEAD
    heads_k = key_width // HEAD
    group = heads_q // heads_k
    blocks = rows_count // WINDOW
    stacked = key_band.reshape(blocks + 2, WINDOW, 2 * key_width)
    joined = jnp.concatenate([stacked[:-2], stacked[1:-1], stacked[2:]], axis=1)
    block_keys = joined[:, :, :key_width].reshape(blocks, 3 * WINDOW, heads_k, HEAD)
    block_values = joined[:, :, key_width:].reshape(blocks, 3 * WINDOW, heads_k, HEAD)
    block_queries = queries.reshape(blocks, WINDOW, heads_k, group, HEAD)
    scores = jnp.einsum(
        "nqhgd,nkhd->nhgqk", block_queries, block_keys, preferred_element_type=jnp.float32
    ) * HEAD ** (-0.5)
    query_pos = positions.reshape(blocks, WINDOW)
    key_pos = query_pos[:, :1] - WINDOW + jnp.arange(3 * WINDOW, dtype=jnp.int32)[None, :]
    inside = (
        (jnp.abs(query_pos[:, :, None] - key_pos[:, None, :]) <= WINDOW)
        & (key_pos[:, None, :] >= 0)
        & (key_pos[:, None, :] < seq)
    )
    scores = jnp.where(inside[:, None, None], scores, neg_big)
    sink = sink_logit.reshape(heads_k, group)[None, :, :, None, None]
    top = jnp.maximum(jnp.max(scores, axis=-1, keepdims=True), sink)
    raised = jnp.exp(scores - top)
    totals = jnp.sum(raised, axis=-1, keepdims=True) + jnp.exp(sink - top)
    weights = (raised / totals).astype(jnp.bfloat16)
    result = jnp.einsum(
        "nhgqk,nkhd->nqhgd", weights, block_values, preferred_element_type=jnp.float32
    )
    return result.astype(jnp.bfloat16).reshape(rows_count, heads_q * HEAD)


def window_pool(pool_band, pool_in, positions, seq):
    rows_count = pool_in.shape[0]
    level = lax.axis_index("tp") * pool_in.shape[1] // (POOL // 4)
    padded = pool_band.astype(jnp.float32)
    sum_two = padded[:-1] + padded[1:]
    sum_four = sum_two[:-2] + sum_two[2:]
    sum_eight = sum_four[:-4] + sum_four[4:]
    sum_sixteen = sum_eight[:-8] + sum_eight[8:]
    candidates = jnp.stack(
        [
            sum_two[7 : 7 + rows_count],
            sum_four[6 : 6 + rows_count],
            sum_eight[4 : 4 + rows_count],
            sum_sixteen[:rows_count],
        ]
    )
    chosen = lax.dynamic_index_in_dim(candidates, level, 0, keepdims=False)
    reach = jnp.left_shift(jnp.int32(1), level)
    low = jnp.clip(positions - reach, 0, seq - 1)
    high = jnp.clip(positions + reach - 1, 0, seq - 1)
    counted = (high - low + 1).astype(jnp.float32)
    return (chosen / counted[:, None]).astype(jnp.bfloat16)


def shards(
    tokens,
    norm_gain,
    w_query,
    w_key,
    w_value,
    w_pool,
    query_gain,
    key_gain,
    sink_logit,
    w_out_pool,
    w_out_attn,
):
    gathered = lax.all_gather(tokens, "tp", axis=1, tiled=True)
    rows_count = gathered.shape[0]
    widened = gathered.astype(jnp.float32)
    normed = (
        widened * lax.rsqrt(jnp.mean(widened * widened, axis=1, keepdims=True) + eps) * norm_gain
    ).astype(jnp.bfloat16)
    positions = lax.axis_index("sp") * rows_count + jnp.arange(rows_count, dtype=jnp.int32)
    seq = lax.axis_size("sp") * rows_count
    cosine, sine = rope_tables(positions, HEAD)
    pieces = sent_together((w_query, w_key, w_value, w_pool), "sp", 0, 1)
    query_raw, key_raw, value_raw, pool_raw = tuple(
        (jnp.dot(normed, piece, preferred_element_type=jnp.float32) for piece in pieces)
    )
    queries = prepare(query_raw, query_gain, cosine, sine)
    keys_new = prepare(key_raw, key_gain, cosine, sine)
    pool_in = pool_raw.astype(jnp.bfloat16)
    key_band = edge_keys(keys_new, value_raw.astype(jnp.bfloat16))
    pool_band = edge_pool(pool_in)
    pooled = window_pool(pool_band, pool_in, positions, seq)
    attended = window_attention(queries, key_band, sink_logit, positions, seq)
    out_pool, out_attn = sent_together((w_out_pool, w_out_attn), "sp", 1, 0)
    return lax.psum_scatter(
        (
            jnp.dot(pooled, out_pool, preferred_element_type=jnp.float32)
            + jnp.dot(attended, out_attn, preferred_element_type=jnp.float32)
        ).astype(jnp.bfloat16),
        "tp",
        scatter_dimension=0,
        tiled=True,
    )


def solution(mesh):
    placed = (
        P("sp", "tp"),
        P(),
        P("sp", "tp"),
        P("sp", "tp"),
        P("sp", "tp"),
        P("sp", "tp"),
        P(),
        P(),
        P("tp"),
        P("tp", "sp"),
        P("tp", "sp"),
    )
    return jax.shard_map(
        shards, mesh=mesh, in_specs=placed, out_specs=P(("sp", "tp"), None), check_vma=False
    )
```

profile of v0, /device:TPU:1, one launch (start us, length us, event | category | flops | bytes accessed | tf_op | source)
XLA Modules:
  0.0 294.5 jit_solution(10621798535016886993)
XLA Ops:
  7.3 1.6 pad_maximum_fusion.7
  9.0 1.5 pad_maximum_fusion.8
  13.5 1.4 fusion.12
  14.9 41.9 %all-gather.4.cloned.1.call-done = bf16[768,4096]{1,0:T(8,128)(2,1)} async-done(((bf16[768,512]{1,0:T(8,128)(2,1)}), bf16[768,4096]{1,0:T(8,128)(2,1)}) %all-gather.4.cloned.1.call-update) | async-done | bytes 6291472 | tf_op jit(solution)/shard_map/all_gather | solution.py:140
  56.8 4.2 %fusion = f32[768]{0:T(1024)S(1)} fusion(bf16[768,4096]{1,0:T(8,128)(2,1)} %all-gather.4.cloned.1.call-done), kind=kLoop, calls=%fused_computation.2 | loop fusion | flops 9436416 | bytes 6294528 | tf_op jit(solution)/shard_map/reduce_sum | solution.py:144
  61.4 5.4 %fusion.2 = bf16[768,4096]{1,0:T(8,128)(2,1)} fusion(bf16[768,4096]{1,0:T(8,128)(2,1)S(1)} %copy-done.1, f32[4096]{0:T(1024)S(1)} %copy-done.3, f32[768]{0:T(1024)S(1)} %add_rsqrt_fusion.2), kind=kLoop, calls=%fused_computation.4 | loop fusion | flops 12582912 | bytes 12602368 | tf_op jit(solution)/shard_map/convert_element_type | solution.py:145
  66.8 74.1 %all-gather.6.cloned.1.call-done = bf16[4096,640]{1,0:T(8,128)(2,1)} async-done(((bf16[128,640]{1,0:T(8,128)(2,1)}), bf16[4096,640]{1,0:T(8,128)(2,1)}) %all-gather.6.cloned.1.call-update) | async-done | bytes 5242896 | tf_op jit(solution)/shard_map/all_gather | solution.py:35
  140.8 5.0 %convolution_convert_fusion.1 = bf16[768,128]{1,0:T(8,128)(2,1)S(1)} fusion(bf16[768,4096]{1,0:T(8,128)(2,1)} %fusion.2, bf16[4096,640]{1,0:T(8,128)(2,1)} %all-gather.6.cloned.1.call-done), kind=kOutput, calls=%fused_computation.26 | convolution fusion | flops 805404672 | bytes 7536640 | tf_op jit(solution)/shard_map/dot_general | solution.py:151
  145.8 1.9 collective-permute-start
  147.7 1.6 collective-permute-start.1
  149.3 3.5 %multiply_reduce_fusion.1 = (f32[768,2]{0,1:T(2,128)S(1)}, f32[768,128]{0,1:T(8,128)S(1)}) fusion(bf16[768,4096]{1,0:T(8,128)(2,1)S(1)} %copy-done, bf16[4096,640]{1,0:T(8,128)(2,1)} %all-gather.6.cloned.1.call-done), kind=kOutput, calls=%fused_computation.74 | convolution fusion | flops 805501440 | bytes 7739392 | tf_op jit(solution)/shard_map/dot_general | solution.py:151
  153.2 2.2 convolution_convert_fusion
  155.4 4.0 %collective-permute-start.2 = (bf16[128,256]{0,1:T(8,128)(2,1)S(1)}, bf16[128,256]{0,1:T(8,128)(2,1)S(1)}, u32[]{:S(2)}, u32[]{:S(2)}) collective-permute-start(bf16[128,256]{0,1:T(8,128)(2,1)S(1)} %get-tuple-element.16), channel_id=1, source_target_pairs={{0,8},{8,16},{16,24},{24,32},{32,40},{40,48},{48,56},{56,64},{64,7... | collective-permute-start | bytes 196616 | tf_op jit(solution)/shard_map/ppermute | solution.py:21
  159.4 1.5 collective-permute-start.3
  160.9 2.0 multiply_reduce_fusion
  164.3 54.8 %all-gather.8.cloned.1.call-done = bf16[384,4096]{1,0:T(8,128)(2,1)} async-done(((bf16[384,128]{1,0:T(8,128)(2,1)}), bf16[384,4096]{1,0:T(8,128)(2,1)}) %all-gather.8.cloned.1.call-update) | async-done | bytes 3145744 | tf_op jit(solution)/shard_map/all_gather | solution.py:35
  219.1 7.6 %fusion.16 = f32[768,4096]{1,0:T(8,128)} fusion(bf16[384,4096]{1,0:T(8,128)(2,1)} %all-gather.8.cloned.1.call-done, s32[]{:T(128)S(6)} %select_n.33, f32[1,768,128]{2,1,0:T(8,128)S(1)} %get-tuple-element.38, f32[1,768,128]{2,1,0:T(8,128)S(1)} %get-tuple-element.39, f32[1,768,128]{2,1,0:T(8,128)S(1)} %get-tuple-element.40, ...), kind=kOutput, calls=%fused_computation.30 | convolution fusion | flops 805797888 | bytes 15207428 | tf_op jit(solution)/shard_map/dot_general | solution.py:163
  228.3 1.0 fusion.4
  229.3 1.0 fusion.3
  230.5 1.4 fusion.10
  232.6 1.3 slice-done.1
  233.9 1.2 slice-done.2
  236.0 4.5 %add_convert_fusion = bf16[768,4096]{1,0:T(8,128)(2,1)} fusion(f32[768,4096]{1,0:T(8,128)S(1)} %bitcast.93, bf16[384,4096]{1,0:T(8,128)(2,1)S(1)} %copy-done.2, bf16[32,8,6,128]{3,2,1,0:T(8,128)(2,1)S(1)} %bitcast.95), kind=kOutput, calls=%fused_computation.5 | convolution fusion | flops 1616904192 | bytes 21495808 | tf_op jit(solution)/shard_map/dot_general | solution.py:164
  240.6 47.4 %reduce-scatter.2.cloned.1.call-done = bf16[96,4096]{1,0:T(8,128)(2,1)} async-done(((bf16[768,4096]{1,0:T(8,128)(2,1)}), bf16[96,4096]{1,0:T(8,128)(2,1)}) %reduce-scatter.2.cloned.1.call-update) | async-done | bytes 786448 | tf_op jit(solution)/shard_map/reduce_scatter | solution.py:161
  (80 shorter events, 9.3 us)
Async XLA Ops:
  6.5 54.5 %copy-start.3 = (f32[4096]{0:T(1024)S(1)}, f32[4096]{0:T(1024)}, u32[]{:S(2)}) copy-start(f32[4096]{0:T(1024)} %param.12) | copy-start | bytes 49156
  6.5 50.3 %all-gather.4.cloned.1.call-start = ((), (), s32[]{:S(2)}) async-start(), calls=%async_computation.1 | async-start | bytes 7077888 | tf_op jit(solution)/shard_map/all_gather | solution.py:140
  7.3 133.6 %all-gather.6.cloned.1.call-start = ((), (), s32[]{:S(2)}) async-start(), calls=%async_computation.2 | async-start | bytes 5406720 | tf_op jit(solution)/shard_map/all_gather | solution.py:35
  8.9 210.1 %all-gather.8.cloned.1.call-start = ((), (), s32[]{:S(2)}) async-start(), calls=%async_computation.3 | async-start | bytes 3244032 | tf_op jit(solution)/shard_map/all_gather | solution.py:35
  10.5 277.5 %reduce-scatter.2.cloned.1.call-start = ((), (), s32[]{:S(2)}) async-start(), calls=%async_computation.4 | async-start | bytes 7077888 | tf_op jit(solution)/shard_map/reduce_scatter | solution.py:161
  56.8 4.6 %copy-start.1 = (bf16[768,4096]{1,0:T(8,128)(2,1)S(1)}, bf16[768,4096]{1,0:T(8,128)(2,1)}, u32[]{:S(2)}) copy-start(bf16[768,4096]{1,0:T(8,128)(2,1)} %all-gather.4.cloned.1.call-done) | copy-start | bytes 18874372
  140.8 8.5 %copy-start = (bf16[768,4096]{1,0:T(8,128)(2,1)S(1)}, bf16[768,4096]{1,0:T(8,128)(2,1)}, u32[]{:S(2)}) copy-start(bf16[768,4096]{1,0:T(8,128)(2,1)} %fusion.2) | copy-start | bytes 18874372
  145.8 18.1 %collective-permute-start = (bf16[8,128]{1,0:T(8,128)(2,1)S(1)}, bf16[8,128]{1,0:T(8,128)(2,1)S(1)}, u32[]{:S(2)}, u32[]{:S(2)}) collective-permute-start(bf16[8,128]{1,0:T(8,128)(2,1)S(1)} %get-tuple-element.22), channel_id=1, source_target_pairs={{0,8},{8,16},{16,24},{24,32},{32,40},{40,48},{48,56},{56,64},{64,7... | collective-permute-start | bytes 6152 | tf_op jit(solution)/shard_map/ppermute | solution.py:21
  147.7 5.4 %slice-start.3 = ((s8[5242880]{0:T(1024)(128)(4,1)}), s8[4194304]{0:T(1024)(128)(4,1)S(1)}, s32[]{:S(2)}) async-start(s8[5242880]{0:T(1024)(128)(4,1)} %bitcast.99), calls=%async_computation.8 | async-start | bytes 8388608
  147.7 5.1 %copy-start.5 = (f32[64]{0:T(128)S(1)}, f32[64]{0:T(128)}, u32[]{:S(2)}) copy-start(f32[64]{0:T(128)} %param.18) | copy-start | bytes 772
  147.7 5.4 %slice-start.4 = ((s8[5242880]{0:T(1024)(128)(4,1)}), s8[1048576]{0:T(1024)(128)(4,1)S(1)}, s32[]{:S(2)}) async-start(s8[5242880]{0:T(1024)(128)(4,1)} %bitcast.99), calls=%async_computation.9 | async-start | bytes 2097152
  147.7 16.2 %collective-permute-start.1 = (bf16[8,128]{1,0:T(8,128)(2,1)S(1)}, bf16[8,128]{1,0:T(8,128)(2,1)S(1)}, u32[]{:S(2)}, u32[]{:S(2)}) collective-permute-start(bf16[8,128]{1,0:T(8,128)(2,1)S(1)} %get-tuple-element.23), channel_id=1, source_target_pairs={{8,0},{16,8},{24,16},{32,24},{40,32},{48,40},{56,48},{64,56},{72,6... | collective-permute-start | bytes 6152 | tf_op jit(solution)/shard_map/ppermute | solution.py:24
  155.4 71.3 %collective-permute-start.2 = (bf16[128,256]{0,1:T(8,128)(2,1)S(1)}, bf16[128,256]{0,1:T(8,128)(2,1)S(1)}, u32[]{:S(2)}, u32[]{:S(2)}) collective-permute-start(bf16[128,256]{0,1:T(8,128)(2,1)S(1)} %get-tuple-element.16), channel_id=1, source_target_pairs={{0,8},{8,16},{16,24},{24,32},{32,40},{40,48},{48,56},{56,64},{64,7... | collective-permute-start | bytes 196616 | tf_op jit(solution)/shard_map/ppermute | solution.py:21
  159.4 3.5 %copy-start.4 = (f32[64]{0:T(128)S(1)}, f32[64]{0:T(128)}, u32[]{:S(2)}) copy-start(f32[64]{0:T(128)} %param.17) | copy-start | bytes 772
  159.4 67.2 %collective-permute-start.3 = (bf16[128,256]{0,1:T(8,128)(2,1)S(1)}, bf16[128,256]{0,1:T(8,128)(2,1)S(1)}, u32[]{:S(2)}, u32[]{:S(2)}) collective-permute-start(bf16[128,256]{0,1:T(8,128)(2,1)S(1)} %get-tuple-element.17), channel_id=1, source_target_pairs={{8,0},{16,8},{24,16},{32,24},{40,32},{48,40},{56,48},{64,56},{72,6... | collective-permute-start | bytes 196616 | tf_op jit(solution)/shard_map/ppermute | solution.py:24
  230.4 2.2 slice-start
  230.5 3.5 %slice-start.1 = ((s8[12582912]{0:T(1024)(128)(4,1)}), s8[4194304]{0:T(1024)(128)(4,1)S(1)}, s32[]{:S(2)}) async-start(s8[12582912]{0:T(1024)(128)(4,1)} %bitcast.92), calls=%async_computation.6 | async-start | bytes 8388608
  230.5 4.6 %slice-start.2 = ((s8[12582912]{0:T(1024)(128)(4,1)}), s8[4194304]{0:T(1024)(128)(4,1)S(1)}, s32[]{:S(2)}) async-start(s8[12582912]{0:T(1024)(128)(4,1)} %bitcast.92), calls=%async_computation.7 | async-start | bytes 8388608
  230.5 5.5 %copy-start.2 = (bf16[384,4096]{1,0:T(8,128)(2,1)S(1)}, bf16[384,4096]{1,0:T(8,128)(2,1)}, u32[]{:S(2)}) copy-start(bf16[384,4096]{1,0:T(8,128)(2,1)} %all-gather.8.cloned.1.call-done) | copy-start | bytes 9437188
Sparse Core Ops, SparseCore 0:
  9.2 47.6 all-gather.3
  59.4 81.3 all-gather.5
  143.3 75.7 all-gather.7
  240.7 47.2 reduce-scatter.1
where the time goes:
time: 295 us
  waiting for transfers between devices  219 us (74%)
  matrix products  27.1 us (9%)
  other arithmetic  17.2 us (6%)
  between operations  13.6 us (5%)
  starting transfers between devices  9 us (3%)
  local copies, waits for them, and re-layouts  8.74 us (3%)
    all_gather x2, waiting for transfers between devices, sent_together(): lax.all_gather(both, axis, axis=dim, tiled=True)  129 us
    reduce_scatter x1, waiting for transfers between devices, shards(): lax.psum_scatter((jnp.dot(pooled, out_pool, preferred_element_type=jnp.fl...  47.4 us
    all_gather x1, waiting for transfers between devices, shards(): gathered = lax.all_gather(tokens, 'tp', axis=1, tiled=True)  41.9 us
    dot_general x4, matrix products, shards(): jnp.dot(normed, piece, preferred_element_type=jnp.float32)  12.7 us
    dot_general x1, matrix products, shards(): jnp.dot(pooled, out_pool, preferred_element_type=jnp.float32)  7.6 us
  transfers between devices with their start and end apart: 8, of which 4 were waited for; matrix products, arithmetic and copies ran while one was open for 13% of the time, Pallas kernels for 0%

commit v1 on v0

--- a/solution.py
+++ b/solution.py
@@ -11,6 +11,12 @@
 rope_base = 10000.0
 neg_big = -1e30
 pool_reach = 8
+
+
+def tiled_gather(x, axis, dim):
+    size = lax.axis_size(axis)
+    repeats = [size if d == dim else 1 for d in range(x.ndim)]
+    return lax.all_to_all(jnp.tile(x, repeats), axis, split_axis=dim, concat_axis=dim, tiled=True)
 
 
 def padded_2(block, sides, width):
@@ -137,7 +143,7 @@
     w_out_pool,
     w_out_attn,
 ):
-    gathered = lax.all_gather(tokens, "tp", axis=1, tiled=True)
+    gathered = tiled_gather(tokens, "tp", 1)
     rows_count = gathered.shape[0]
     widened = gathered.astype(jnp.float32)
     normed = (

time: 295 us -> 254 us (0.86)
  waiting for transfers between devices: 219 us -> 143 us
  local copies, waits for them, and re-layouts: 8.74 us -> 26.3 us
  starting transfers between devices: 9 us -> 16.2 us
  other arithmetic: 17.2 us -> 22.3 us
  matrix products: 27.1 us -> 31.9 us
    all_gather x2, waiting for transfers between devices: 129 us -> 27.9 us  [sent_together(): lax.all_gather(both, axis, axis=dim, tiled=True)]
    all_to_all x0 -> x1, waiting for transfers between devices: none -> 67.5 us  [tiled_gather(): lax.all_to_all(jnp.tile(x, repeats), axis, split_axis=dim, concat_axis=di...]
    all_gather x1 -> x0, waiting for transfers between devices: 41.9 us -> none  [shards(): gathered = lax.all_gather(tokens, 'tp', axis=1, tiled=True)]
    all_to_all x0 -> x1, local copies, waits for them, and re-layouts: none -> 8.66 us  [tiled_gather(): lax.all_to_all(jnp.tile(x, repeats), axis, split_axis=dim, concat_axis=di...]
    all_to_all x0 -> x1, starting transfers between devices: none -> 7.99 us  [tiled_gather(): lax.all_to_all(jnp.tile(x, repeats), axis, split_axis=dim, concat_axis=di...]
    dot_general x0 -> x4, local copies, waits for them, and re-layouts: none -> 5.74 us  [shards(): jnp.dot(normed, piece, preferred_element_type=jnp.float32)]
    another operation x0 -> x1, local copies, waits for them, and re-layouts: none -> 4.3 us  [tiled_gather(): jnp.tile(x, repeats)]
    convert_element_type x1 -> x2, other arithmetic: 5.36 us -> 8.24 us  [shards(): normed = (widened * lax.rsqrt(jnp.mean(widened * widened, axis=1, keepdim...]
  transfers between devices with their start and end apart: 8 -> 8, of which waited for: 4 -> 3; matrix products, arithmetic and copies ran while one was open for 13% -> 24% of each run, Pallas kernels for 0% -> 0%
where the time goes in v1:
time: 254 us; the launch traced here: 253 us
  waiting for transfers between devices  143 us (56%)
  matrix products  31.9 us (13%)
  local copies, waits for them, and re-layouts  26.3 us (10%)
  other arithmetic  22.3 us (9%)
  starting transfers between devices  16.2 us (6%)
  between operations  13.6 us (5%)
    all_to_all x1, waiting for transfers between devices, tiled_gather(): lax.all_to_all(jnp.tile(x, repeats), axis, split_axis=dim, concat_axis=di...  67.5 us
    reduce_scatter x1, waiting for transfers between devices, shards(): lax.psum_scatter((jnp.dot(pooled, out_pool, preferred_element_type=jnp.fl...  47.5 us
    all_gather x2, waiting for transfers between devices, sent_together(): lax.all_gather(both, axis, axis=dim, tiled=True)  27.9 us
    dot_general x4, matrix products, shards(): jnp.dot(normed, piece, preferred_element_type=jnp.float32)  15 us
    all_to_all x1, local copies, waits for them, and re-layouts, tiled_gather(): lax.all_to_all(jnp.tile(x, repeats), axis, split_axis=dim, concat_axis=di...  8.66 us
    convert_element_type x2, other arithmetic, shards(): normed = (widened * lax.rsqrt(jnp.mean(widened * widened, axis=1, keepdim...  8.24 us
    all_to_all x1, starting transfers between devices, tiled_gather(): lax.all_to_all(jnp.tile(x, repeats), axis, split_axis=dim, concat_axis=di...  7.99 us
    dot_general x1, matrix products, shards(): jnp.dot(pooled, out_pool, preferred_element_type=jnp.float32)  7.59 us
  transfers between devices with their start and end apart: 8, of which 3 were waited for; matrix products, arithmetic and copies ran while one was open for 24% of the time, Pallas kernels for 0%

profile of v1, /device:TPU:1, one launch (start us, length us, event | category | flops | bytes accessed | tf_op | source)
XLA Modules:
  0.0 253.3 jit_solution(7823903011190737706)
XLA Ops:
  6.5 1.6 pad_maximum_fusion.7
  8.1 4.3 %tile.2 = bf16[768,8,512]{2,0,1:T(8,128)(2,1)} broadcast(bf16[768,512]{1,0:T(8,128)(2,1)} %param.11), dimensions={0,2} | broadcast | bytes 7077888 | tf_op jit(solution)/shard_map/tile | solution.py:19
  12.4 8.0 %all-to-all-start = ((bf16[768,8,512]{2,0,1:T(8,128)(2,1)}), bf16[768,8,512]{2,0,1:T(8,128)(2,1)}, u32[]{:S(2)}, u32[]{:S(2)}) async-start(bf16[768,8,512]{2,0,1:T(8,128)(2,1)} %tile.2), calls=%async_computation | async-start | bytes 12582912 | tf_op jit(solution)/shard_map/all_to_all | solution.py:19
  22.9 1.4 fusion.9
  24.3 67.5 %all-to-all-done = bf16[768,8,512]{2,0,1:T(8,128)(2,1)} async-done(((bf16[768,8,512]{2,0,1:T(8,128)(2,1)}), bf16[768,8,512]{2,0,1:T(8,128)(2,1)}, u32[]{:S(2)}, u32[]{:S(2)}) %all-to-all-start) | async-done | bytes 6291488 | tf_op jit(solution)/shard_map/all_to_all | solution.py:19
  91.7 8.7 %copy.68 = bf16[768,8,512]{0,2,1:T(8,128)(2,1)} copy(bf16[768,8,512]{2,0,1:T(8,128)(2,1)} %all-to-all-done) | data formatting | bytes 12582912 | tf_op jit(solution)/shard_map/all_to_all | solution.py:19
  100.4 4.2 %multiply_reduce_fusion = f32[768]{0:T(1024)S(1)} fusion(bf16[768,8,512]{0,2,1:T(8,128)(2,1)} %copy.68), kind=kLoop, calls=%fused_computation.5 | loop fusion | flops 9436416 | bytes 6294528 | tf_op jit(solution)/shard_map/reduce_sum | solution.py:150
  105.0 4.1 %fusion.1 = bf16[768,4096]{0,1:T(8,128)(2,1)} fusion(bf16[768,8,512]{0,2,1:T(8,128)(2,1)S(1)} %copy-done, f32[4096]{0:T(1024)S(1)} %copy-done.7, f32[768]{0:T(1024)S(1)} %add_rsqrt_fusion.2), kind=kLoop, calls=%fused_computation.2 | loop fusion | flops 12582912 | bytes 12602368 | tf_op jit(solution)/shard_map/convert_element_type | solution.py:151
  109.1 4.1 %multiply_convert_fusion = bf16[768,8,512]{0,2,1:T(8,128)(2,1)} fusion(bf16[768,8,512]{0,2,1:T(8,128)(2,1)S(1)} %copy-done, f32[8,512]{1,0:T(8,128)S(1)} %mul.166, f32[768]{0:T(1024)S(1)} %add_rsqrt_fusion.2), kind=kLoop, calls=%fused_computation.4 | loop fusion | flops 12582912 | bytes 12602368 | tf_op jit(solution)/shard_map/convert_element_type | solution.py:151
  114.5 1.3 copy.69
  115.9 4.2 %multiply_reduce_fusion.2 = (f32[768,2]{0,1:T(2,128)S(1)}, f32[768,2,64]{0,2,1:T(8,128)S(1)}) fusion(bf16[768,4096,1]{0,1,2:T(8,128)(2,1)} %bitcast.79, bf16[2,64,4096]{2,1,0:T(8,128)(2,1)} %bitcast.91), kind=kOutput, calls=%fused_computation.66 | convolution fusion | flops 805501440 | bytes 7739392 | tf_op jit(solution)/shard_map/dot_general | solution.py:157
  120.3 1.6 fusion.25
  123.1 1.4 collective-permute-start.2
  126.0 3.0 %copy.76 = bf16[256,4096]{1,0:T(8,128)(2,1)} copy(bf16[256,4096]{0,1:T(8,128)(2,1)S(1)} %slice_bitcast_fusion) | data formatting | bytes 4194304 | tf_op jit(solution)/shard_map/dot_general | solution.py:157
  129.0 5.0 %convolution_convert_fusion.1 = bf16[768,128]{1,0:T(8,128)(2,1)S(1)} fusion(bf16[768,4096]{0,1:T(8,128)(2,1)} %fusion.1, bf16[4096,640]{1,0:T(8,128)(2,1)} %all-gather.3.cloned.1.call-done), kind=kOutput, calls=%fused_computation.25 | convolution fusion | flops 805404672 | bytes 7536640 | tf_op jit(solution)/shard_map/dot_general | solution.py:157
  134.0 4.0 %collective-permute-start = (bf16[8,128]{1,0:T(8,128)(2,1)S(1)}, bf16[8,128]{1,0:T(8,128)(2,1)S(1)}, u32[]{:S(2)}, u32[]{:S(2)}) collective-permute-start(bf16[8,128]{1,0:T(8,128)(2,1)S(1)} %get-tuple-element.22), channel_id=1, source_target_pairs={{0,8},{8,16},{16,24},{24,32},{32,40},{40,48},{48,56},{56,64},{64,7... | collective-permute-start | bytes 6152 | tf_op jit(solution)/shard_map/ppermute | solution.py:27
  138.0 1.5 collective-permute-start.1
  139.5 4.7 %multiply_reduce_fusion.1 = (f32[768,4]{0,1:T(4,128)S(1)}, f32[768,4,64]{0,2,1:T(8,128)S(1)}) fusion(bf16[768,4096,1]{0,1,2:T(8,128)(2,1)} %bitcast.80, bf16[4,64,4096]{2,1,0:T(8,128)(2,1)S(1)} %bitcast.84), kind=kOutput, calls=%fused_computation.35 | convolution fusion | flops 1611002880 | bytes 9187328 | tf_op jit(solution)/shard_map/dot_general | solution.py:157
  145.6 27.9 %all-gather.5.cloned.1.call-done = bf16[384,4096]{1,0:T(8,128)(2,1)} async-done(((bf16[384,128]{1,0:T(8,128)(2,1)}), bf16[384,4096]{1,0:T(8,128)(2,1)}) %all-gather.5.cloned.1.call-update) | async-done | bytes 3145744 | tf_op jit(solution)/shard_map/all_gather | solution.py:41
  173.5 7.6 %fusion.11 = f32[768,4096]{1,0:T(8,128)} fusion(bf16[384,4096]{1,0:T(8,128)(2,1)} %all-gather.5.cloned.1.call-done, s32[]{:T(128)S(6)} %select_n.33, f32[1,768,128]{2,1,0:T(8,128)S(1)} %get-tuple-element.38, f32[1,768,128]{2,1,0:T(8,128)S(1)} %get-tuple-element.39, f32[1,768,128]{2,1,0:T(8,128)S(1)} %get-tuple-element.40, ...), kind=kOutput, calls=%fused_computation.28 | convolution fusion | flops 805797888 | bytes 15207428 | tf_op jit(solution)/shard_map/dot_general | solution.py:169
  184.3 2.0 copy-done.1
  187.8 3.8 %fusion.7 = bf16[6,128,2,2,64]{1,4,3,2,0:T(8,128)(2,1)S(1)} fusion(bf16[6,384,2,64,1]{1,3,4,2,0:T(8,128)(2,1)S(1)} %bitcast.92, f32[6,2,384,128,2]{3,2,4,1,0:T(8,128)} %copy-done.1, f32[6,2,2,128]{3,2,1,0:T(2,128)S(1)} %exponential_add_fusion, f32[6,2,2,128]{3,2,1,0:T(2,128)S(1)} %broadcast_maximum_fusion, pred[6,128,384]{1,2,0:T(8,128)(4,1)S(1)} %fusion.9), kind=kOutput, calls=%fused_computation.19 | convolution fusion | flops 157089792 | bytes 6021120 | tf_op jit(solution)/shard_map/nhgqk,nkhd->nqhgd/dot_general | solution.py:103
  194.8 4.5 %add_convert_fusion = bf16[768,4096]{1,0:T(8,128)(2,1)} fusion(f32[768,4096]{1,0:T(8,128)S(1)} %bitcast.78, bf16[384,4096]{1,0:T(8,128)(2,1)S(1)} %copy-done.2, bf16[32,8,6,128]{3,2,1,0:T(8,128)(2,1)S(1)} %bitcast.87), kind=kOutput, calls=%fused_computation.3 | convolution fusion | flops 1616904192 | bytes 21495808 | tf_op jit(solution)/shard_map/dot_general | solution.py:170
  199.3 47.5 %reduce-scatter.2.cloned.1.call-done = bf16[96,4096]{1,0:T(8,128)(2,1)} async-done(((bf16[768,4096]{1,0:T(8,128)(2,1)}), bf16[96,4096]{1,0:T(8,128)(2,1)}) %reduce-scatter.2.cloned.1.call-update) | async-done | bytes 786448 | tf_op jit(solution)/shard_map/reduce_scatter | solution.py:167
  (95 shorter events, 15.8 us)
Async XLA Ops:
  6.5 106.7 %all-gather.3.cloned.1.call-start = ((), (), s32[]{:S(2)}) async-start(), calls=%async_computation.2 | async-start | bytes 5406720 | tf_op jit(solution)/shard_map/all_gather | solution.py:41
  12.4 8.0 %copy-start.8 = (bf16[256,128]{1,0:T(8,128)(2,1)S(1)}, bf16[256,128]{1,0:T(8,128)(2,1)}, u32[]{:S(2)}) copy-start(bf16[256,128]{1,0:T(8,128)(2,1)} %param.21) | copy-start | bytes 196612
  12.4 8.0 %copy-start.9 = (bf16[128,128]{1,0:T(8,128)(2,1)S(1)}, bf16[128,128]{1,0:T(8,128)(2,1)}, u32[]{:S(2)}) copy-start(bf16[128,128]{1,0:T(8,128)(2,1)} %param.20) | copy-start | bytes 98308
  12.4 8.8 %copy-start.7 = (f32[4096]{0:T(1024)S(1)}, f32[4096]{0:T(1024)}, u32[]{:S(2)}) copy-start(f32[4096]{0:T(1024)} %param.12) | copy-start | bytes 49156
  12.4 8.8 %copy-start.12 = (f32[4]{0:T(128)S(1)}, f32[4]{0:T(128)}, u32[]{:S(2)}) copy-start(f32[4]{0:T(128)} %param.19) | copy-start | bytes 52
  12.4 79.3 %all-to-all-start = ((bf16[768,8,512]{2,0,1:T(8,128)(2,1)}), bf16[768,8,512]{2,0,1:T(8,128)(2,1)}, u32[]{:S(2)}, u32[]{:S(2)}) async-start(bf16[768,8,512]{2,0,1:T(8,128)(2,1)} %tile.2), calls=%async_computation | async-start | bytes 12582912 | tf_op jit(solution)/shard_map/all_to_all | solution.py:19
  20.4 153.1 %all-gather.5.cloned.1.call-start = ((), (), s32[]{:S(2)}) async-start(), calls=%async_computation.3 | async-start | bytes 3244032 | tf_op jit(solution)/shard_map/all_gather | solution.py:41
  21.2 225.6 %reduce-scatter.2.cloned.1.call-start = ((), (), s32[]{:S(2)}) async-start(), calls=%async_computation.4 | async-start | bytes 7077888 | tf_op jit(solution)/shard_map/reduce_scatter | solution.py:167
  100.4 4.6 %copy-start = (bf16[768,8,512]{0,2,1:T(8,128)(2,1)S(1)}, bf16[768,8,512]{0,2,1:T(8,128)(2,1)}, u32[]{:S(2)}) copy-start(bf16[768,8,512]{0,2,1:T(8,128)(2,1)} %copy.68) | copy-start | bytes 18874372
  114.5 5.6 %copy-start.10 = (f32[64]{0:T(128)S(1)}, f32[64]{0:T(128)}, u32[]{:S(2)}) copy-start(f32[64]{0:T(128)} %param.18) | copy-start | bytes 772
  114.5 7.3 %slice-start.3 = ((s8[6291456]{0:T(1024)(128)(4,1)}), s8[2097152]{0:T(1024)(128)(4,1)S(1)}, s32[]{:S(2)}) async-start(s8[6291456]{0:T(1024)(128)(4,1)} %bitcast.81), calls=%async_computation.8 | async-start | bytes 4194304
  115.9 4.4 %copy-start.5 = (f32[768,64]{0,1:T(8,128)S(1)}, f32[768,64]{0,1:T(8,128)}, u32[]{:S(2)}) copy-start(f32[768,64]{0,1:T(8,128)} %get-tuple-element.24) | copy-start | bytes 589828
  115.9 6.0 %slice-start.4 = ((s8[6291456]{0:T(1024)(128)(4,1)}), s8[4194304]{0:T(1024)(128)(4,1)S(1)}, s32[]{:S(2)}) async-start(s8[6291456]{0:T(1024)(128)(4,1)} %bitcast.81), calls=%async_computation.9 | async-start | bytes 8388608
  115.9 6.1 %copy-start.4 = (bf16[4096,640]{1,0:T(8,128)(2,1)S(1)}, bf16[4096,640]{1,0:T(8,128)(2,1)}, u32[]{:S(2)}) copy-start(bf16[4096,640]{1,0:T(8,128)(2,1)} %all-gather.3.cloned.1.call-done) | copy-start | bytes 15728644
  123.1 58.0 %collective-permute-start.2 = (bf16[128,256]{0,1:T(8,128)(2,1)S(1)}, bf16[128,256]{0,1:T(8,128)(2,1)S(1)}, u32[]{:S(2)}, u32[]{:S(2)}) collective-permute-start(bf16[128,256]{0,1:T(8,128)(2,1)S(1)} %get-tuple-element.16), channel_id=1, source_target_pairs={{0,8},{8,16},{16,24},{24,32},{32,40},{40,48},{48,56},{56,64},{64,7... | collective-permute-start | bytes 196616 | tf_op jit(solution)/shard_map/ppermute | solution.py:27
  124.6 56.6 %collective-permute-start.3 = (bf16[128,256]{0,1:T(8,128)(2,1)S(1)}, bf16[128,256]{0,1:T(8,128)(2,1)}, u32[]{:S(2)}, u32[]{:S(2)}) collective-permute-start(bf16[128,256]{0,1:T(8,128)(2,1)S(1)} %get-tuple-element.17), channel_id=1, source_target_pairs={{8,0},{16,8},{24,16},{32,24},{40,32},{48,40},{56,48},{64,56},{72,6... | collective-permute-start | bytes 196616 | tf_op jit(solution)/shard_map/ppermute | solution.py:30
  129.0 10.5 %copy-start.3 = (bf16[256,4096]{1,0:T(8,128)(2,1)S(1)}, bf16[256,4096]{1,0:T(8,128)(2,1)}, u32[]{:S(2)}) copy-start(bf16[256,4096]{1,0:T(8,128)(2,1)} %copy.76) | copy-start | bytes 6291460
  134.0 11.2 %collective-permute-start = (bf16[8,128]{1,0:T(8,128)(2,1)S(1)}, bf16[8,128]{1,0:T(8,128)(2,1)S(1)}, u32[]{:S(2)}, u32[]{:S(2)}) collective-permute-start(bf16[8,128]{1,0:T(8,128)(2,1)S(1)} %get-tuple-element.22), channel_id=1, source_target_pairs={{0,8},{8,16},{16,24},{24,32},{32,40},{40,48},{48,56},{56,64},{64,7... | collective-permute-start | bytes 6152 | tf_op jit(solution)/shard_map/ppermute | solution.py:27
  138.0 7.2 %collective-permute-start.1 = (bf16[8,128]{1,0:T(8,128)(2,1)S(1)}, bf16[8,128]{1,0:T(8,128)(2,1)S(1)}, u32[]{:S(2)}, u32[]{:S(2)}) collective-permute-start(bf16[8,128]{1,0:T(8,128)(2,1)S(1)} %get-tuple-element.23), channel_id=1, source_target_pairs={{8,0},{16,8},{24,16},{32,24},{40,32},{48,40},{56,48},{64,56},{72,6... | collective-permute-start | bytes 6152 | tf_op jit(solution)/shard_map/ppermute | solution.py:30
  139.5 4.7 %copy-start.11 = (f32[64]{0:T(128)S(1)}, f32[64]{0:T(128)}, u32[]{:S(2)}) copy-start(f32[64]{0:T(128)} %param.17) | copy-start | bytes 772
  139.5 4.9 %copy-start.6 = (f32[768,64]{0,1:T(8,128)S(1)}, f32[768,64]{0,1:T(8,128)}, u32[]{:S(2)}) copy-start(f32[768,64]{0,1:T(8,128)} %get-tuple-element.25) | copy-start | bytes 589828
  187.8 4.9 %slice-start.1 = ((s8[12582912]{0:T(1024)(128)(4,1)}), s8[4194304]{0:T(1024)(128)(4,1)S(1)}, s32[]{:S(2)}) async-start(s8[12582912]{0:T(1024)(128)(4,1)} %bitcast.77), calls=%async_computation.6 | async-start | bytes 8388608
  187.8 6.1 %slice-start.2 = ((s8[12582912]{0:T(1024)(128)(4,1)}), s8[4194304]{0:T(1024)(128)(4,1)S(1)}, s32[]{:S(2)}) async-start(s8[12582912]{0:T(1024)(128)(4,1)} %bitcast.77), calls=%async_computation.7 | async-start | bytes 8388608
  187.8 7.0 %copy-start.2 = (bf16[384,4096]{1,0:T(8,128)(2,1)S(1)}, bf16[384,4096]{1,0:T(8,128)(2,1)}, u32[]{:S(2)}) copy-start(bf16[384,4096]{1,0:T(8,128)(2,1)} %all-gather.5.cloned.1.call-done) | copy-start | bytes 9437188
  (2 other events, 6.3 us)
Sparse Core Ops, SparseCore 0:
  9.9 85.4 all-gather.2
  97.8 75.6 all-gather.4
  199.4 47.3 reduce-scatter.1
